TPU v7x, 32 devices: a whole 2x2x4 slice. The times are simulated.
32 devices in a mesh: kv: 8 (over z, y), tp: 4 (over x, core).
Axes of the slice: x: 2, y: 2, z: 4, core: 2. Of those that a mesh axis runs over, the one named last changes fastest.
Arguments:
- piece_tokens: bfloat16 [32, 2048], P('kv'), may hold values from -6 to 6
- decode_tokens: bfloat16 [8, 2048], P('kv'), may hold values from -6 to 6
- prompt_fill: int32 [1], replicated, may hold values from 1024 to 2016
- decode_fill: int32 [8], P('kv'), may hold values from 1 to 767, 3072 in all
- prompt_cache: bfloat16 [2048, 544], P('kv'), may hold values from -600 to 600
- decode_cache: bfloat16 [8, 768, 544], P('kv'), may hold values from -600 to 600
- input_gain: float32 [2048], replicated, may hold values from 0.1 to 1.9
- query_gain: float32 [768], replicated, may hold values from 0.1 to 1.9
- latent_gain: float32 [512], replicated, may hold values from 0.1 to 1.9
- query_down: bfloat16 [2048, 768], P(None, 'tp'), may hold values from -0.125 to 0.125
- latent_down: bfloat16 [2048, 512], P(None, 'tp'), may hold values from -0.125 to 0.125
- rope_down: bfloat16 [2048, 32], replicated, may hold values from -0.125 to 0.125
- query_up: bfloat16 [768, 1024], P(None, 'tp'), may hold values from -0.21875 to 0.21875
- qrope_up: bfloat16 [768, 512], P(None, 'tp'), may hold values from -0.21875 to 0.21875
- key_up: bfloat16 [16, 64, 512], P('tp'), may hold values from -0.25 to 0.25
- value_up: bfloat16 [16, 512, 64], P('tp'), may hold values from -4 to 4
- out_proj: bfloat16 [1024, 2048], P('tp'), may hold values from -4 to 4
Outputs:
- piece_out: bfloat16 [32, 2048], P('kv')
- decode_out: bfloat16 [8, 2048], P('kv')
- piece_rows: bfloat16 [32, 544], P('kv')
- decode_rows: bfloat16 [8, 544], P('kv')
Inputs may be any that keep to these rules, and one draw needn't show every extreme that they name: `prompt_fill`: the piece takes the 32 positions that follow the cache's filled positions. `decode_fill`: a decoding sequence's new token takes the position that follows its filled ones.
All inputs are finite; a program needn't handle non-finite values. No bound on the sum of `decode_fill` on one device may be relied on, other than what follows from the above.
Results may differ from a plain program's by a relative error of at most 0.035.
Values may be sent and summed in bfloat16 or wider, within the bound.
A program may use at most 64 MiB of HBM per device.

v0:
```python
import jax
import jax.numpy as jnp
from jax import lax
from jax.sharding import PartitionSpec as P

NOPE = 64
ROPE = 32


NEG_FILL = -1e30
RMS_EPS = 1e-06
THETA = 10000.0


def rms_scale(values, gain_row):
    widened = values.astype(jnp.float32)
    scaled = (
        widened
        * lax.rsqrt(jnp.mean(widened * widened, axis=-1, keepdims=True) + RMS_EPS)
        * gain_row
    )
    return scaled.astype(jnp.bfloat16)


def rotate(values, places):
    half_width = values.shape[-1] // 2
    inverse = THETA ** (-jnp.arange(half_width, dtype=jnp.float32) / half_width)
    angles = places.astype(jnp.float32)[..., None] * inverse
    first_half = values[..., :half_width].astype(jnp.float32)
    second_half = values[..., half_width:].astype(jnp.float32)
    cosine = jnp.cos(angles)
    sine_part = jnp.sin(angles)
    return jnp.concatenate(
        [
            first_half * cosine - second_half * sine_part,
            first_half * sine_part + second_half * cosine,
        ],
        axis=-1,
    ).astype(jnp.bfloat16)


def make_queries(query_lat, places, query_up, qrope_up, key_up):
    row_count = query_lat.shape[0]
    head_count = key_up.shape[0]
    nope_part = (
        jnp.dot(query_lat, query_up, preferred_element_type=jnp.float32)
        .astype(jnp.bfloat16)
        .reshape(row_count, head_count, -1)
    )
    rope_raw = (
        jnp.dot(query_lat, qrope_up, preferred_element_type=jnp.float32)
        .astype(jnp.bfloat16)
        .reshape(row_count, head_count, -1)
    )
    turned = rotate(rope_raw, places[:, None])
    absorbed = jnp.einsum(
        "nhc,hcl->nhl", nope_part, key_up, preferred_element_type=jnp.float32
    ).astype(jnp.bfloat16)
    return (absorbed, turned)


def block_attend(absorbed, turned, key_rows, key_places, query_places, value_up):
    latent_width = value_up.shape[1]
    score_scale = (NOPE + ROPE) ** (-0.5)
    latent_keys = key_rows[:, :latent_width]
    scores = (
        jnp.einsum("nhl,sl->nhs", absorbed, latent_keys, preferred_element_type=jnp.float32)
        + jnp.einsum(
            "nhr,sr->nhs", turned, key_rows[:, latent_width:], preferred_element_type=jnp.float32
        )
    ) * score_scale
    allowed = key_places[None, None, :] <= query_places[:, None, None]
    scores = jnp.where(allowed, scores, NEG_FILL)
    local_peak = jnp.max(scores, axis=-1)
    exp_scores = jnp.where(allowed, jnp.exp(scores - local_peak[..., None]), 0.0)
    weight_sum = jnp.sum(exp_scores, axis=-1)
    weights = exp_scores.astype(jnp.bfloat16)
    mixed_rows = jnp.einsum("nhs,sl->nhl", weights, latent_keys, preferred_element_type=jnp.float32)
    partial_sum = jnp.einsum(
        "nhl,hlv->nhv", mixed_rows, value_up.astype(jnp.float32), precision=lax.Precision.HIGHEST
    )
    return (partial_sum, weight_sum, local_peak)


def insert_row(cache_rows, new_row, fill_one):
    return lax.dynamic_update_slice(cache_rows, new_row[None], (fill_one, jnp.zeros((), jnp.int32)))


def local(
    piece_tokens,
    decode_tokens,
    prompt_fill,
    decode_fill,
    prompt_cache,
    decode_cache,
    input_gain,
    query_gain,
    latent_gain,
    query_down,
    latent_down,
    rope_down,
    query_up,
    qrope_up,
    key_up,
    value_up,
    out_proj,
):
    kv_index = lax.axis_index("kv")
    piece_dev = piece_tokens.shape[0]
    shard_len = prompt_cache.shape[0]
    fill_start = prompt_fill[0]
    own_places = fill_start + kv_index * piece_dev + jnp.arange(piece_dev, dtype=jnp.int32)
    places = jnp.concatenate([own_places, decode_fill])
    tokens = jnp.concatenate([piece_tokens, decode_tokens], axis=0)
    normed = rms_scale(tokens, input_gain)
    query_comp = jnp.dot(normed, query_down, preferred_element_type=jnp.float32).astype(
        jnp.bfloat16
    )
    latent_comp = jnp.dot(normed, latent_down, preferred_element_type=jnp.float32).astype(
        jnp.bfloat16
    )
    query_comp, latent_comp = (
        lax.all_gather(query_comp, "tp", axis=1, tiled=True),
        lax.all_gather(latent_comp, "tp", axis=1, tiled=True),
    )
    query_lat = rms_scale(query_comp, query_gain)
    rope_raw = jnp.dot(normed, rope_down, preferred_element_type=jnp.float32).astype(jnp.bfloat16)
    new_rows = jnp.concatenate(
        [rms_scale(latent_comp, latent_gain), rotate(rope_raw, places)], axis=-1
    )
    piece_rows = new_rows[:piece_dev]
    decode_rows = new_rows[piece_dev:]
    decode_absorbed, decode_turned = make_queries(
        query_lat[piece_dev:], decode_fill, query_up, qrope_up, key_up
    )
    piece_latent, arrived = (
        lax.all_gather(query_lat[:piece_dev], "kv", axis=0, tiled=True),
        lax.all_gather(piece_rows, "kv", axis=0, tiled=True),
    )
    arrived_places = fill_start + jnp.arange(arrived.shape[0], dtype=jnp.int32)
    piece_absorbed, piece_turned = make_queries(
        piece_latent, arrived_places, query_up, qrope_up, key_up
    )
    piece_total = arrived.shape[0]
    query_places = fill_start + jnp.arange(piece_total, dtype=jnp.int32)
    zero_rows = jnp.zeros((shard_len, arrived.shape[1]), arrived.dtype)
    padded = jnp.concatenate([zero_rows, arrived, zero_rows], axis=0)
    offset = jnp.clip(kv_index * shard_len - fill_start + shard_len, 0, piece_total + shard_len)
    window = lax.dynamic_slice_in_dim(padded, offset, shard_len, 0)
    key_places = kv_index * shard_len + jnp.arange(shard_len, dtype=jnp.int32)
    fresh_rows = (key_places >= fill_start) & (key_places < fill_start + piece_total)
    key_rows = jnp.where(fresh_rows[:, None], window, prompt_cache)
    partial_sum, weight_sum, local_peak = block_attend(
        piece_absorbed, piece_turned, key_rows, key_places, query_places, value_up
    )
    all_parts, all_totals, all_peaks = (
        lax.all_to_all(
            partial_sum.reshape(1, piece_total, -1), "kv", split_axis=1, concat_axis=0, tiled=True
        ),
        lax.all_to_all(weight_sum[None], "kv", split_axis=1, concat_axis=0, tiled=True),
        lax.all_to_all(local_peak[None], "kv", split_axis=1, concat_axis=0, tiled=True),
    )
    global_peak = jnp.max(all_peaks, axis=0)
    factor = jnp.exp(all_peaks - global_peak[None])
    merged = jnp.sum(all_parts.reshape(all_peaks.shape + (-1,)) * factor[..., None], axis=0)
    denominator = jnp.sum(all_totals * factor, axis=0)
    piece_value = (merged / denominator[..., None]).astype(jnp.bfloat16)
    decode_keys = jax.vmap(insert_row)(decode_cache, decode_rows, decode_fill)

    def attend_one(absorbed_one, turned_one, keys_one, fill_one):
        cache_places = jnp.arange(keys_one.shape[0], dtype=jnp.int32)
        return block_attend(
            absorbed_one[None], turned_one[None], keys_one, cache_places, fill_one[None], value_up
        )

    decode_part, decode_total, decode_peak = jax.vmap(attend_one)(
        decode_absorbed, decode_turned, decode_keys, decode_fill
    )
    decode_value = (decode_part[:, 0] / decode_total[:, 0, :, None]).astype(jnp.bfloat16)
    values = jnp.concatenate([piece_value, decode_value], axis=0)
    values = values.reshape(values.shape[0], -1)
    partial_value = jnp.dot(values, out_proj, preferred_element_type=jnp.float32).astype(
        jnp.bfloat16
    )
    summed = lax.psum(partial_value, "tp").astype(jnp.float32).astype(jnp.bfloat16)
    return (summed[:piece_dev], summed[piece_dev:], piece_rows, decode_rows)


def solution(mesh):
    placed = (
        P("kv", None),
        P("kv", None),
        P(),
        P("kv"),
        P("kv", None),
        P("kv", None, None),
        P(),
        P(),
        P(),
        P(None, "tp"),
        P(None, "tp"),
        P(),
        P(None, "tp"),
        P(None, "tp"),
        P("tp", None, None),
        P("tp", None, None),
        P("tp", None),
    )
    return jax.shard_map(
        local,
        mesh=mesh,
        in_specs=placed,
        out_specs=(P("kv", None), P("kv", None), P("kv", None), P("kv", None)),
        check_vma=False,
    )
```

profile of v0, /device:TPU:0, one launch (start us, length us, event | category | flops | bytes accessed | tf_op | source)
XLA Modules:
  0.0 135.7 jit_solution(8345209168863359578)
XLA Ops:
  0.7 1.3 copy.80
  4.0 6.2 %all_gather.14 = bf16[5,512]{1,0:T(8,128)(2,1)S(1)} all-gather(bf16[5,128]{1,0:T(8,128)(2,1)S(1)} %convolution_convert_fusion.5), channel_id=1, replica_groups=mesh['kv'=8,'tp'=4] {'tp'}, dimensions={1}, use_global_device_ids=true | all-gather | bytes 6400 | tf_op jit(solution)/shard_map/all_gather | solution.py:124
  10.3 0.3 fusion.5
  10.6 5.5 %all-gather = bf16[4,192,5]{1,2,0:T(8,128)(2,1)S(1)} all-gather(bf16[1,192,5]{1,2,0:T(8,128)(2,1)S(1)} %fusion.5), channel_id=1, replica_groups=mesh['kv'=8,'tp'=4] {'tp'}, dimensions={0}, use_global_device_ids=true | all-gather | bytes 9600 | tf_op jit(solution)/shard_map/all_gather | solution.py:123
  16.7 0.6 copy-done.12
  17.6 31.4 %all-gather.2 = bf16[8,4,544]{2,1,0:T(4,128)(2,1)S(1)} all-gather(bf16[1,4,544]{2,1,0:T(4,128)(2,1)S(1)} %slice_bitcast_fusion.14), channel_id=1, replica_groups=mesh['kv'=8,'tp'=4] {'kv'}, dimensions={0}, use_global_device_ids=true | all-gather | bytes 39168 | tf_op jit(solution)/shard_map/all_gather | solution.py:138
  49.2 30.8 %all-gather.1 = bf16[8,4,768]{2,1,0:T(4,128)(2,1)S(1)} all-gather(bf16[1,4,768]{2,1,0:T(4,128)(2,1)S(1)} %slice_bitcast_fusion.10), channel_id=1, replica_groups=mesh['kv'=8,'tp'=4] {'kv'}, dimensions={0}, use_global_device_ids=true | all-gather | bytes 55296 | tf_op jit(solution)/shard_map/all_gather | solution.py:137
  80.9 0.9 fusion.10
  81.9 0.7 copy-done.2
  82.7 0.4 fusion.76
  83.2 0.7 copy.46
  83.9 5.4 %all-to-all-start.2 = ((f32[1,32,4]{2,0,1:T(1,128)}), f32[1,32,4]{2,0,1:T(1,128)S(1)}, u32[]{:S(2)}, u32[]{:S(2)}) async-start(f32[1,32,4]{2,0,1:T(1,128)} %copy.46), calls=%async_computation.2 | async-start | bytes 32768 | tf_op jit(solution)/shard_map/all_to_all | solution.py:160
  89.9 0.6 copy-done.14
  90.7 0.6 fusion.74
  91.3 0.8 constant_dynamic-slice_fusion
  92.1 0.7 copy-done.13
  92.8 2.0 %and_reduce_fusion = pred[]{:T(512)} fusion(s32[3]{0:T(128)S(1)} %copy-done.13, s32[1]{0:T(128)} %bitcast.20, s32[1]{0:T(128)} %bitcast.19, s32[1]{0:T(128)} %constant.79.clone.1), kind=kLoop, calls=%fused_computation.108 | loop fusion | flops 17 | bytes 25 | tf_op jit(solution)/shard_map/reduce.1
  94.8 1.2 broadcast_select_fusion
  96.2 1.6 %scatter.4 = bf16[1,768,544]{1,2,0:T(8,128)(2,1)S(1)} dynamic-update-slice(bf16[1,768,544]{1,2,0:T(8,128)(2,1)S(1)} %copy.80, bf16[1,1,544]{1,2,0:T(8,128)(2,1)S(1)} %copy.50, s32[]{:T(128)} %constant.75.clone.1, s32[]{:T(128)} %bitcast.22, s32[]{:T(128)} %constant.75.clone.1) | dynamic-update-slice | bytes 2180 | tf_op jit(solution)/shard_map/vmap(vmap())/scatter | solution.py:86
  98.5 0.3 fusion.75
  99.1 0.6 copy-done.7
  100.1 0.3 convolution_bitcast_fusion
  100.6 0.7 copy.43
  101.3 6.0 %all-to-all-start.1 = ((f32[1,32,4]{2,0,1:T(1,128)}), f32[1,32,4]{2,0,1:T(1,128)S(1)}, u32[]{:S(2)}, u32[]{:S(2)}) async-start(f32[1,32,4]{2,0,1:T(1,128)} %copy.43), calls=%async_computation.1 | async-start | bytes 32768 | tf_op jit(solution)/shard_map/all_to_all | solution.py:161
  107.4 0.6 slice.96
  108.1 0.7 reshape.442
  109.0 4.9 %all-to-all-done.1 = f32[1,32,4]{2,0,1:T(1,128)S(1)} async-done(((f32[1,32,4]{2,0,1:T(1,128)}), f32[1,32,4]{2,0,1:T(1,128)S(1)}, u32[]{:S(2)}, u32[]{:S(2)}) %all-to-all-start.1) | async-done | bytes 544 | tf_op jit(solution)/shard_map/all_to_all | solution.py:161
  113.9 3.3 %all-to-all-start = ((f32[1,32,256]{2,0,1:T(1,128)}), f32[1,32,256]{2,0,1:T(1,128)S(1)}, u32[]{:S(2)}, u32[]{:S(2)}) async-start(f32[1,32,256]{2,0,1:T(1,128)} %reshape.442), calls=%async_computation | async-start | bytes 65536 | tf_op jit(solution)/shard_map/all_to_all | solution.py:157
  118.1 5.7 %all-to-all-done = f32[1,32,256]{2,0,1:T(1,128)S(1)} async-done(((f32[1,32,256]{2,0,1:T(1,128)}), f32[1,32,256]{2,0,1:T(1,128)S(1)}, u32[]{:S(2)}, u32[]{:S(2)}) %all-to-all-start) | async-done | bytes 32800 | tf_op jit(solution)/shard_map/all_to_all | solution.py:157
  124.2 10.3 %psum.7 = bf16[5,2048]{1,0:T(8,128)(2,1)S(1)} all-reduce(bf16[5,2048]{1,0:T(8,128)(2,1)S(1)} %convolution_convert_fusion), channel_id=1, replica_groups=mesh['kv'=8,'tp'=4] {'tp'}, use_global_device_ids=true, to_apply=%region_11.12 | all-reduce | flops 10240 | bytes 40960 | tf_op jit(solution)/shard_map/psum | solution.py:185
  134.5 0.6 slice.104
  135.1 0.6 slice.105
  (99 shorter events, 6.9 us)
Async XLA Ops:
  0.6 123.3 %copy-start = (bf16[256,2048]{1,0:T(8,128)(2,1)S(1)}, bf16[256,2048]{1,0:T(8,128)(2,1)}, u32[]{:S(2)}) copy-start(bf16[256,2048]{1,0:T(8,128)(2,1)} %param.35) | copy-start | bytes 3145732
  0.6 3.1 %copy-start.5 = (bf16[2048,128]{1,0:T(8,128)(2,1)S(1)}, bf16[2048,128]{1,0:T(8,128)(2,1)}, u32[]{:S(2)}) copy-start(bf16[2048,128]{1,0:T(8,128)(2,1)} %param.29) | copy-start | bytes 1572868
  0.7 2.9 %copy-start.15 = (bf16[2048,32]{0,1:T(8,128)(2,1)S(1)}, bf16[2048,32]{0,1:T(8,128)(2,1)}, u32[]{:S(2)}) copy-start(bf16[2048,32]{0,1:T(8,128)(2,1)} %param.30) | copy-start | bytes 393220
  0.7 2.7 %copy-start.8 = (bf16[4,2048]{1,0:T(4,128)(2,1)S(1)}, bf16[4,2048]{1,0:T(4,128)(2,1)}, u32[]{:S(2)}) copy-start(bf16[4,2048]{1,0:T(4,128)(2,1)} %param.19) | copy-start | bytes 49156
  0.7 2.7 %copy-start.9 = (bf16[1,2048]{1,0:T(2,128)(2,1)S(1)}, bf16[1,2048]{1,0:T(2,128)(2,1)}, u32[]{:S(2)}) copy-start(bf16[1,2048]{1,0:T(2,128)(2,1)} %param.20) | copy-start | bytes 12292
  0.7 2.9 %copy-start.10 = (f32[2048]{0:T(1024)S(1)}, f32[2048]{0:T(1024)}, u32[]{:S(2)}) copy-start(f32[2048]{0:T(1024)} %param.25) | copy-start | bytes 24580
  2.0 8.3 %copy-start.3 = (bf16[2048,192]{0,1:T(8,128)(2,1)S(1)}, bf16[2048,192]{0,1:T(8,128)(2,1)}, u32[]{:S(2)}) copy-start(bf16[2048,192]{0,1:T(8,128)(2,1)} %param.28) | copy-start | bytes 2359300
  10.3 6.1 %copy-start.6 = (bf16[256,544]{0,1:T(8,128)(2,1)S(1)}, bf16[256,544]{0,1:T(8,128)(2,1)}, u32[]{:S(2)}) copy-start(bf16[256,544]{0,1:T(8,128)(2,1)} %param.23) | copy-start | bytes 835588
  16.6 0.7 copy-start.12
  17.3 31.8 %copy-start.11 = (f32[768]{0:T(1024)S(1)}, f32[768]{0:T(1024)}, u32[]{:S(2)}) copy-start(f32[768]{0:T(1024)} %param.26) | copy-start | bytes 9220
  17.5 62.5 %copy-start.4 = (bf16[768,128]{1,0:T(8,128)(2,1)S(1)}, bf16[768,128]{1,0:T(8,128)(2,1)}, u32[]{:S(2)}) copy-start(bf16[768,128]{1,0:T(8,128)(2,1)} %param.32) | copy-start | bytes 589828
  17.5 62.8 %copy-start.1 = (bf16[768,256]{1,0:T(8,128)(2,1)S(1)}, bf16[768,256]{1,0:T(8,128)(2,1)}, u32[]{:S(2)}) copy-start(bf16[768,256]{1,0:T(8,128)(2,1)} %param.31) | copy-start | bytes 1179652
  81.7 1.0 copy-start.2
  83.9 17.4 %all-to-all-start.2 = ((f32[1,32,4]{2,0,1:T(1,128)}), f32[1,32,4]{2,0,1:T(1,128)S(1)}, u32[]{:S(2)}, u32[]{:S(2)}) async-start(f32[1,32,4]{2,0,1:T(1,128)} %copy.46), calls=%async_computation.2 | async-start | bytes 32768 | tf_op jit(solution)/shard_map/all_to_all | solution.py:160
  89.9 0.7 copy-start.14
  92.1 0.7 copy-start.13
  98.8 1.0 copy-start.7
  101.3 12.6 %all-to-all-start.1 = ((f32[1,32,4]{2,0,1:T(1,128)}), f32[1,32,4]{2,0,1:T(1,128)S(1)}, u32[]{:S(2)}, u32[]{:S(2)}) async-start(f32[1,32,4]{2,0,1:T(1,128)} %copy.43), calls=%async_computation.1 | async-start | bytes 32768 | tf_op jit(solution)/shard_map/all_to_all | solution.py:161
  113.9 10.0 %all-to-all-start = ((f32[1,32,256]{2,0,1:T(1,128)}), f32[1,32,256]{2,0,1:T(1,128)S(1)}, u32[]{:S(2)}, u32[]{:S(2)}) async-start(f32[1,32,256]{2,0,1:T(1,128)} %reshape.442), calls=%async_computation | async-start | bytes 65536 | tf_op jit(solution)/shard_map/all_to_all | solution.py:157
where the time goes:
time: 136 us
  blocking collectives  84.1 us (62%)
  starting transfers between devices  14.8 us (11%)
  local copies, waits for them, and re-layouts  13.7 us (10%)
  waiting for transfers between devices  10.7 us (8%)
  other arithmetic  5.93 us (4%)
  matrix products  4.06 us (3%)
  between operations  2.43 us (2%)
    all_gather x1, blocking collectives, local(): lax.all_gather(piece_rows, 'kv', axis=0, tiled=True)  31.4 us
    all_gather x1, blocking collectives, local(): lax.all_gather(query_lat[:piece_dev], 'kv', axis=0, tiled=True)  30.8 us
    psum x1, blocking collectives, local(): lax.psum(partial_value, 'tp').astype(jnp.float32).astype(jnp.bfloat16)  10.3 us
    all_gather x1, blocking collectives, local(): lax.all_gather(latent_comp, 'tp', axis=1, tiled=True)  6.16 us
    all_to_all x1, starting transfers between devices, local(): lax.all_to_all(local_peak[None], 'kv', split_axis=1, concat_axis=0, tiled...  6 us
    all_to_all x1, waiting for transfers between devices, local(): lax.all_to_all(partial_sum.reshape(1, piece_total, -1), 'kv', split_axis=...  5.73 us
    all_gather x1, blocking collectives, local(): lax.all_gather(query_comp, 'tp', axis=1, tiled=True)  5.5 us
    all_to_all x1, starting transfers between devices, local(): lax.all_to_all(weight_sum[None], 'kv', split_axis=1, concat_axis=0, tiled...  5.43 us
  transfers between devices with their start and end apart: 3, of which 2 were waited for; matrix products, arithmetic and copies ran while one was open for 9% of the time, Pallas kernels for 0%

commit v1 on v0

v1 whole, which is shorter than its diff:
```python
import functools
import math

import jax
import jax.numpy as jnp
from jax import lax
from jax.experimental import pallas as pl
from jax.experimental.pallas import tpu as pltpu
from jax.sharding import PartitionSpec as P

NOPE = 64
ROPE = 32
NEG_FILL = -1e30
RMS_EPS = 1e-06
THETA = 10000.0
F32 = jnp.float32
BF16 = jnp.bfloat16
MESH = pl.DeviceIdType.MESH


def dot(a, b):
    return jnp.dot(a, b, preferred_element_type=F32)


def dot_t(a, b):
    return lax.dot_general(a, b, (((1,), (1,)), ((), ())), preferred_element_type=F32)


def round_up(value, step):
    return -(-value // step) * step


def kernel(
    n,
    m,
    pt_h,
    dt_h,
    pfill,
    dfill,
    pc_h,
    dc_h,
    ig_h,
    qg_h,
    lg_h,
    qd_h,
    ld_h,
    rd_h,
    qu_h,
    ru_h,
    ku_h,
    vu_h,
    op_h,
    po_ref,
    do_ref,
    pr_ref,
    dr_ref,
    tok,
    dtok,
    kbuf,
    dbuf,
    ig,
    qg,
    lg,
    qd,
    ld,
    rd,
    qu,
    ru,
    ku,
    vu,
    op,
    x,
    qx,
    lx,
    csend,
    crecv,
    vbuf,
    obuf,
    in_sem,
    tok_sem,
    a_sem,
    l_sem,
    c_sem,
    o_sem,
):
    me = lax.axis_index("kv")
    mt = lax.axis_index("tp")
    p = tok.shape[1]
    dd = dtok.shape[0]
    width = tok.shape[2]
    own = vbuf.shape[0]
    rows = x.shape[0]
    cache = pc_h.shape[0]
    slots = dc_h.shape[1]
    heads = ku.shape[0]
    kl = ku.shape[2]
    key_width = kbuf.shape[1]
    part_q = qd.shape[1]
    ql = qu.shape[0]
    extra = kbuf.shape[0] - cache
    chunk = obuf.shape[3]
    chunks = obuf.shape[1]

    pairs = [
        (pt_h, tok.at[0]),
        (dt_h, dtok),
        (ig_h, ig),
        (qd_h, qd),
        (ld_h, ld),
        (rd_h, rd),
        (qg_h, qg),
        (lg_h, lg),
        (qu_h, qu),
        (ru_h, ru),
        (ku_h, ku),
        (pc_h, kbuf.at[pl.ds(0, cache)]),
        (vu_h, vu),
        (dc_h, dbuf.at[:, pl.ds(0, slots)]),
        (op_h, op),
    ]
    loads = [pltpu.make_async_copy(s, d, in_sem.at[i]) for i, (s, d) in enumerate(pairs)]
    for load in loads:
        load.start()
    l_pt, l_dt, l_ig, l_qd, l_ld, l_rd, l_qg, l_lg, l_qu, l_ru, l_ku, l_pc, l_vu, l_dc, l_op = loads

    barrier = pltpu.get_barrier_semaphore()
    for d in range(1, n):
        pl.semaphore_signal(
            barrier, inc=1, device_id=(lax.rem(me + d, n), mt), device_id_type=MESH
        )
    for d in range(1, m):
        pl.semaphore_signal(
            barrier, inc=1, device_id=(me, lax.rem(mt + d, m)), device_id_type=MESH
        )
    l_pt.wait()
    pl.semaphore_wait(barrier, n - 1 + m - 1)

    tok_copies = []
    for d in range(1, n):
        copy = pltpu.make_async_remote_copy(
            src_ref=tok.at[0],
            dst_ref=tok.at[d],
            send_sem=tok_sem.at[0, d],
            recv_sem=tok_sem.at[1, d],
            device_id=(lax.rem(me + d, n), mt),
            device_id_type=MESH,
        )
        copy.start()
        tok_copies.append(copy)

    fill = pfill[0]
    row = lax.broadcasted_iota(jnp.int32, (rows, 1), 0)
    slot = jnp.zeros((rows, 1), jnp.int32)
    for d in range(1, n):
        slot = jnp.where(row >= own + (d - 1) * p, d, slot)
    source = me - slot
    source = jnp.where(source < 0, source + n, source)
    inside = jnp.where(slot == 0, row, row - own - (slot - 1) * p)
    places = fill + source * p + inside
    for b in range(dd):
        places = jnp.where(row == p + b, dfill[b], places)
    half = ROPE // 2
    lane = lax.broadcasted_iota(jnp.int32, (1, heads * ROPE), 1)
    frequency = jnp.zeros((1, heads * ROPE), F32)
    for i in range(half):
        frequency = jnp.where(lane % half == i, THETA ** (-i / half), frequency)
    angles = places.astype(F32) * frequency
    cosine = jnp.cos(angles)
    sine = jnp.sin(angles)

    x[...] = jnp.zeros_like(x)
    x[0:p, :] = tok[0].astype(F32)
    l_dt.wait()
    x[p : p + dd, :] = dtok[...].astype(F32)
    l_ig.wait()
    l_qd.wait()
    l_ld.wait()
    l_rd.wait()
    for d in range(1, n):
        tok_copies[d - 1].wait_recv()
        start = own + (d - 1) * p
        x[start : start + p, :] = tok[d].astype(F32)
    xs = x[...]
    normed = (
        xs * lax.rsqrt(jnp.mean(xs * xs, axis=-1, keepdims=True) + RMS_EPS) * ig[...]
    ).astype(BF16)
    qx[mt] = dot(normed, qd[...]).astype(BF16)
    lx[mt] = dot(normed[0:extra], ld[...]).astype(BF16)

    a_copies = []
    for d in range(1, m):
        peer = (me, lax.rem(mt + d, m))
        for buf, sem in ((qx, a_sem), (lx, l_sem)):
            copy = pltpu.make_async_remote_copy(
                src_ref=buf.at[mt],
                dst_ref=buf.at[mt],
                send_sem=sem.at[0, d],
                recv_sem=sem.at[1, d],
                device_id=peer,
                device_id_type=MESH,
            )
            copy.start()
            a_copies.append(copy)

    raw = dot(normed[0:extra], rd[...]).astype(BF16).astype(F32)
    cos_own = cosine[0:extra, 0:half]
    sin_own = sine[0:extra, 0:half]
    first, second = raw[:, 0:half], raw[:, half:ROPE]
    new_rope = jnp.concatenate(
        [first * cos_own - second * sin_own, first * sin_own + second * cos_own], axis=1
    )
    for load in (l_qg, l_lg, l_qu, l_ru, l_ku, l_pc, l_vu, l_dc):
        load.wait()
    gains = qg[...]
    for copy in a_copies:
        copy.wait_recv()

    parts = [qx[s].astype(F32) for s in range(m)]
    square = sum(jnp.sum(v * v, axis=-1, keepdims=True) for v in parts)
    scale = lax.rsqrt(square / ql + RMS_EPS)
    nope = jnp.zeros((rows, qu.shape[1]), F32)
    turn = jnp.zeros((rows, ru.shape[1]), F32)
    for s in range(m):
        lat = (parts[s] * scale * gains[:, s * part_q : (s + 1) * part_q]).astype(BF16)
        nope += dot(lat, qu[s * part_q : (s + 1) * part_q, :])
        turn += dot(lat, ru[s * part_q : (s + 1) * part_q, :])
    nope = nope.astype(BF16)
    turn = turn.astype(BF16).astype(F32)
    turned_axis = heads * ROPE
    above = pltpu.roll(turn, turned_axis - half, 1)
    below = pltpu.roll(turn, half, 1)
    turned = turn * cosine + jnp.where(lane % ROPE < half, -above, below) * sine
    nd = qu.shape[1] // heads
    absorbed = [dot(nope[:, h * nd : (h + 1) * nd], ku[h]) for h in range(heads)]
    turned = [turned[:, h * ROPE : (h + 1) * ROPE] for h in range(heads)]

    latent = jnp.concatenate([lx[s].astype(F32) for s in range(m)], axis=1)
    latent = (
        latent * lax.rsqrt(jnp.mean(latent * latent, axis=-1, keepdims=True) + RMS_EPS) * lg[...]
    )
    new_rows = jnp.concatenate([latent, new_rope], axis=1)
    new_bf = new_rows.astype(BF16)
    kbuf[cache : cache + extra, :] = new_bf
    pr_ref[...] = new_rows[0:p].astype(BF16)
    dr_ref[...] = new_rows[p : p + dd].astype(BF16)

    score_scale = (NOPE + ROPE) ** (-0.5)
    aq = jnp.concatenate([v.astype(BF16) for v in absorbed], axis=0)
    tq = jnp.concatenate([v.astype(BF16) for v in turned], axis=0)
    scores = (dot_t(aq, kbuf[:, 0:kl]) + dot_t(tq, kbuf[:, kl:key_width])) * score_scale
    key = lax.broadcasted_iota(jnp.int32, scores.shape, 1)
    query_place = jnp.concatenate([places] * heads, axis=0)
    fresh = key - cache
    key_place = jnp.where(fresh < 0, me * cache + key, fill + me * p + fresh)
    limit = jnp.where(fresh < 0, jnp.minimum(fill - 1, query_place), query_place)
    allowed = (key_place <= limit) & (fresh < p)
    scores = jnp.where(allowed, scores, NEG_FILL)
    peak = jnp.max(scores, axis=-1, keepdims=True)
    weights = jnp.where(allowed, jnp.exp(scores - peak), 0.0)
    total = jnp.sum(weights, axis=-1, keepdims=True)
    mixed = dot(weights.astype(BF16), kbuf[:, 0:kl]).astype(BF16)
    vd = vu.shape[2]
    stat_lane = lax.broadcasted_iota(jnp.int32, (rows, crecv.shape[2] - vd), 1)
    for h in range(heads):
        cut = slice(h * rows, (h + 1) * rows)
        stats = jnp.where(stat_lane == 0, total[cut], peak[cut])
        message = jnp.concatenate([dot(mixed[cut], vu[h]), stats], axis=1)
        csend[0, h * p : (h + 1) * p, :] = message[0:p]
        for d in range(1, n):
            start = own + (d - 1) * p
            csend[d, h * p : (h + 1) * p, :] = message[start : start + p]

    c_copies = []
    for d in range(1, n):
        copy = pltpu.make_async_remote_copy(
            src_ref=csend.at[d],
            dst_ref=crecv.at[d],
            send_sem=c_sem.at[0, d],
            recv_sem=c_sem.at[1, d],
            device_id=(lax.rem(me + n - d, n), mt),
            device_id_type=MESH,
        )
        copy.start()
        c_copies.append(copy)

    vbuf[...] = jnp.zeros_like(vbuf)
    for b in range(dd):
        dbuf[b, slots : slots + extra, :] = new_bf
        at = slice(p + b, p + b + 1)
        qa = jnp.concatenate([v[at] for v in absorbed], axis=0).astype(BF16)
        qt = jnp.concatenate([v[at] for v in turned], axis=0).astype(BF16)
        ds = (dot_t(qa, dbuf[b, :, 0:kl]) + dot_t(qt, dbuf[b, :, kl:key_width])) * score_scale
        dk = lax.broadcasted_iota(jnp.int32, ds.shape, 1)
        ok = (dk < jnp.minimum(dfill[b], slots)) | (dk == slots + p + b)
        ds = jnp.where(ok, ds, NEG_FILL)
        dpeak = jnp.max(ds, axis=-1, keepdims=True)
        dw = jnp.where(ok, jnp.exp(ds - dpeak), 0.0)
        dtotal = jnp.sum(dw, axis=-1, keepdims=True)
        dmix = dot(dw.astype(BF16), dbuf[b, :, 0:kl]).astype(BF16)
        dvals = [dot(dmix, vu[h])[h : h + 1] / dtotal[h : h + 1] for h in range(heads)]
        vbuf[p + b : p + b + 1, :] = jnp.concatenate(dvals, axis=1)
    l_op.wait()

    for copy in c_copies:
        copy.wait_recv()
    blocks = [csend[0]] + [crecv[d] for d in range(1, n)]
    top = blocks[0][:, vd + 1 : vd + 2]
    for block in blocks[1:]:
        top = jnp.maximum(top, block[:, vd + 1 : vd + 2])
    merged = jnp.zeros(blocks[0].shape, F32)
    for block in blocks:
        merged += block * jnp.exp(block[:, vd + 1 : vd + 2] - top)
    value = merged[:, 0:vd] / merged[:, vd : vd + 1]
    vbuf[0:p, :] = jnp.concatenate([value[h * p : (h + 1) * p] for h in range(heads)], axis=1)
    values = vbuf[...].astype(BF16)

    o_copies = []
    for c in range(chunks):
        obuf[mt, c] = dot(values, op[:, c * chunk : (c + 1) * chunk]).astype(BF16)
        for d in range(1, m):
            copy = pltpu.make_async_remote_copy(
                src_ref=obuf.at[mt, c],
                dst_ref=obuf.at[mt, c],
                send_sem=o_sem.at[0, d, c],
                recv_sem=o_sem.at[1, d, c],
                device_id=(me, lax.rem(mt + d, m)),
                device_id_type=MESH,
            )
            copy.start()
            o_copies.append(copy)
    for copy in o_copies:
        copy.wait_recv()
    for c in range(chunks):
        out = sum(obuf[s, c].astype(F32) for s in range(m))
        po_ref[:, c * chunk : (c + 1) * chunk] = out[0:p].astype(BF16)
        do_ref[:, c * chunk : (c + 1) * chunk] = out[p : p + dd].astype(BF16)
    for copy in tok_copies + a_copies + c_copies + o_copies:
        copy.wait_send()


def local(n, m, *args):
    (pt, dt, pfill, dfill, pc, dc, ig, qg, lg, qd, ld, rd, qu, ru, ku, vu, op) = args
    p, width = pt.shape
    dd = dt.shape[0]
    own = round_up(p + dd, 8)
    rows = round_up(own + (n - 1) * p, 16)
    extra = round_up(own, 16)
    heads, nd, kl = ku.shape
    chunks = 2
    any_spec = pl.BlockSpec(memory_space=pl.ANY)
    smem = pl.BlockSpec(memory_space=pltpu.SMEM)
    vmem = pl.BlockSpec(memory_space=pltpu.VMEM)
    ig, qg, lg = ig[None], qg[None], lg[None]
    like = lambda a: pltpu.VMEM(a.shape, a.dtype)
    scratch = [
        pltpu.VMEM((n, p, width), BF16),
        like(dt),
        pltpu.VMEM((pc.shape[0] + extra, pc.shape[1]), BF16),
        pltpu.VMEM((dd, dc.shape[1] + extra, dc.shape[2]), BF16),
        *[like(a) for a in (ig, qg, lg, qd, ld, rd, qu, ru, ku, vu, op)],
        pltpu.VMEM((rows, width), F32),
        pltpu.VMEM((m, rows, qd.shape[1]), BF16),
        pltpu.VMEM((m, extra, ld.shape[1]), BF16),
        pltpu.VMEM((n, heads * p, 128), F32),
        pltpu.VMEM((n, heads * p, 128), F32),
        pltpu.VMEM((own, op.shape[0]), F32),
        pltpu.VMEM((m, chunks, own, width // chunks), BF16),
        pltpu.SemaphoreType.DMA((15,)),
        pltpu.SemaphoreType.DMA((2, n)),
        pltpu.SemaphoreType.DMA((2, m)),
        pltpu.SemaphoreType.DMA((2, m)),
        pltpu.SemaphoreType.DMA((2, n)),
        pltpu.SemaphoreType.DMA((2, m, chunks)),
    ]
    return pl.pallas_call(
        functools.partial(kernel, n, m),
        out_shape=(
            jax.ShapeDtypeStruct((p, width), BF16),
            jax.ShapeDtypeStruct((dd, width), BF16),
            jax.ShapeDtypeStruct((p, pc.shape[1]), BF16),
            jax.ShapeDtypeStruct((dd, pc.shape[1]), BF16),
        ),
        in_specs=[any_spec, any_spec, smem, smem] + [any_spec] * 13,
        out_specs=(vmem,) * 4,
        scratch_shapes=scratch,
        compiler_params=pltpu.CompilerParams(
            collective_id=0, has_side_effects=True, vmem_limit_bytes=60 * 1024 * 1024
        ),
    )(pt, dt, pfill, dfill, pc, dc, ig, qg, lg, qd, ld, rd, qu, ru, ku, vu, op)


def solution(mesh):
    placed = (
        P("kv", None),
        P("kv", None),
        P(),
        P("kv"),
        P("kv", None),
        P("kv", None, None),
        P(),
        P(),
        P(),
        P(None, "tp"),
        P(None, "tp"),
        P(),
        P(None, "tp"),
        P(None, "tp"),
        P("tp", None, None),
        P("tp", None, None),
        P("tp", None),
    )
    return jax.shard_map(
        functools.partial(local, mesh.shape["kv"], mesh.shape["tp"]),
        mesh=mesh,
        in_specs=placed,
        out_specs=(P("kv", None), P("kv", None), P("kv", None), P("kv", None)),
        check_vma=False,
    )
```

time: 136 us -> 37.8 us (0.28)
  blocking collectives: 84.1 us -> 0 us
  Pallas kernels: 0 us -> 25.1 us
  starting transfers between devices: 14.8 us -> 0 us
  waiting for transfers between devices: 10.7 us -> 0 us
  other arithmetic: 5.93 us -> 0 us
  matrix products: 4.06 us -> 0 us
  local copies, waits for them, and re-layouts: 13.7 us -> 10.4 us
    all_gather x4 -> x0, blocking collectives: 73.8 us -> none  [the longest x1 31.4 us: local(): lax.all_gather(piece_rows, 'kv', axis=0, tiled=True)]
    pallas_call x0 -> x1, Pallas kernels: none -> 25.1 us  [local(): pl.pallas_call(functools.partial(kernel, n, m), out_shape=(jax.ShapeDtype...]
    all_to_all x3 -> x0, starting transfers between devices: 14.8 us -> none  [the longest x1 6 us: local(): lax.all_to_all(local_peak[None], 'kv', split_axis=1, concat_axis=0, tiled...]
    all_to_all x3 -> x0, waiting for transfers between devices: 10.7 us -> none  [the longest x1 5.73 us: local(): lax.all_to_all(partial_sum.reshape(1, piece_total, -1), 'kv', split_axis=...]
    psum x1 -> x0, blocking collectives: 10.3 us -> none  [local(): lax.psum(partial_value, 'tp').astype(jnp.float32).astype(jnp.bfloat16)]
    unnamed x40 -> x25, local copies, waits for them, and re-layouts: 5.09 us -> 9.81 us
    dot_general x17 -> x0, matrix products: 4.06 us -> none  [the longest x2 0.64 us: block_attend(): jnp.einsum('nhl,hlv->nhv', mixed_rows, value_up.astype(jnp.float32), prec...]
    another operation x4 -> x0, other arithmetic: 3.34 us -> none
  transfers between devices with their start and end apart: 3 -> 0, of which waited for: 2 -> 0; matrix products, arithmetic and copies ran while one was open for 9% -> 0% of each run, Pallas kernels for 0% -> 0%
where the time goes in v1:
time: 37.8 us; the launch traced here: 37.4 us
  Pallas kernels  25.1 us (66%)
  local copies, waits for them, and re-layouts  10.4 us (28%)
  between operations  1.98 us (5%)
    pallas_call x1, Pallas kernels, local(): pl.pallas_call(functools.partial(kernel, n, m), out_shape=(jax.ShapeDtype...  25.1 us
    unnamed x25, local copies, waits for them, and re-layouts  9.81 us

profile of v1, /device:TPU:0, one launch (start us, length us, event | category | flops | bytes accessed | tf_op | source)
XLA Modules:
  0.0 37.4 jit_solution(2803571723707375654)
XLA Ops:
  0.6 0.0 copy-start.6
  1.9 0.0 copy-done.6
  2.0 0.6 %broadcast_in_dim.10.qg_h = f32[1,768]{1,0:T(1,128)} reshape(f32[768]{0:T(1024)S(1)} %copy-done.6) | data formatting | bytes 6144 | tf_op jit(solution)/shard_map/broadcast_in_dim | solution.py:353
  2.5 0.0 copy-start.3
  2.5 0.0 copy-start.2
  2.5 1.9 %copy.21.pc_h = bf16[256,544]{1,0:T(8,128)(2,1)} copy(bf16[256,544]{0,1:T(8,128)(2,1)} %param.21) | data formatting | bytes 557056 | tf_op args[4]
  4.4 0.0 copy-done.3
  4.5 0.0 copy-start
  4.5 1.0 %copy.24.rd_h = bf16[2048,32]{1,0:T(8,128)(2,1)} copy(bf16[2048,32]{0,1:T(8,128)(2,1)S(1)} %copy-done.3) | data formatting | bytes 262144 | tf_op args[11]
  5.5 0.0 copy-done.2
  5.5 1.0 %copy.25.vu_h = bf16[4,512,64]{2,1,0:T(8,128)(2,1)} copy(bf16[4,512,64]{1,2,0:T(8,128)(2,1)S(1)} %copy-done.2) | data formatting | bytes 524288 | tf_op args[15]
  6.5 0.0 copy-done
  6.5 0.0 copy-start.1
  6.5 1.3 %copy.22.dc_h = bf16[1,768,544]{2,1,0:T(8,128)(2,1)} copy(bf16[1,768,544]{1,2,0:T(8,128)(2,1)S(1)} %copy-done) | data formatting | bytes 1671168 | tf_op args[5]
  7.8 0.0 copy-done.1
  7.8 1.3 %copy.23.qd_h = bf16[2048,192]{1,0:T(8,128)(2,1)} copy(bf16[2048,192]{0,1:T(8,128)(2,1)S(1)} %copy-done.1) | data formatting | bytes 1572864 | tf_op args[9]
  9.1 25.1 %shard_map.192 = (bf16[4,2048]{1,0:T(4,128)(2,1)}, bf16[1,2048]{1,0:T(2,128)(2,1)}, bf16[4,544]{1,0:T(4,128)(2,1)}, bf16[1,544]{1,0:T(2,128)(2,1)}) custom-call(bf16[4,2048]{1,0:T(4,128)(2,1)} %pt_h.1, bf16[1,2048]{1,0:T(2,128)(2,1)} %dt_h.1, s32[1]{0:T(128)S(6)} %copy.30.pfill, s32[1]{0:T(128)S(6)} %copy.31.dfill, bf16[256,544]{1,0:T(8,128)(2,1)} %copy.21.pc_h, ...), custom_call_target="tpu_custom_call" | custom-call | tf_op jit(solution)/shard_map/pallas_call | solution.py:375
  34.1 0.0 copy-start.4
  34.2 1.3 %copy.32 = bf16[4,2048]{1,0:T(4,128)(2,1)} copy(bf16[4,2048]{1,0:T(4,128)(2,1)} %get-tuple-element.8) | data formatting | bytes 32768
  35.5 0.0 copy-done.4
  35.5 0.0 copy-start.5
  35.5 0.6 %copy.33 = bf16[1,2048]{1,0:T(2,128)(2,1)} copy(bf16[1,2048]{1,0:T(2,128)(2,1)S(1)} %copy-done.4) | data formatting | bytes 8192
  36.1 0.1 copy-done.5
  36.2 0.0 copy-start.7
  36.2 0.6 %copy.34 = bf16[4,544]{1,0:T(4,128)(2,1)} copy(bf16[4,544]{1,0:T(4,128)(2,1)S(1)} %copy-done.5) | data formatting | bytes 8704
  36.8 0.1 copy-done.7
  36.8 0.6 %copy.35 = bf16[1,544]{1,0:T(2,128)(2,1)} copy(bf16[1,544]{1,0:T(2,128)(2,1)S(1)} %copy-done.7) | data formatting | bytes 2176
Async XLA Ops:
  0.6 1.3 %copy-start.6 = (f32[768]{0:T(1024)S(1)}, f32[768]{0:T(1024)}, u32[]{:S(2)}) copy-start(f32[768]{0:T(1024)} %param.24) | copy-start | bytes 9220
  2.5 1.9 %copy-start.3 = (bf16[2048,32]{0,1:T(8,128)(2,1)S(1)}, bf16[2048,32]{0,1:T(8,128)(2,1)}, u32[]{:S(2)}) copy-start(bf16[2048,32]{0,1:T(8,128)(2,1)} %param.28) | copy-start | bytes 393220
  2.5 2.9 %copy-start.2 = (bf16[4,512,64]{1,2,0:T(8,128)(2,1)S(1)}, bf16[4,512,64]{1,2,0:T(8,128)(2,1)}, u32[]{:S(2)}) copy-start(bf16[4,512,64]{1,2,0:T(8,128)(2,1)} %param.32) | copy-start | bytes 786436
  4.5 2.0 %copy-start = (bf16[1,768,544]{1,2,0:T(8,128)(2,1)S(1)}, bf16[1,768,544]{1,2,0:T(8,128)(2,1)}, u32[]{:S(2)}) copy-start(bf16[1,768,544]{1,2,0:T(8,128)(2,1)} %param.22) | copy-start | bytes 2506756
  6.5 1.3 %copy-start.1 = (bf16[2048,192]{0,1:T(8,128)(2,1)S(1)}, bf16[2048,192]{0,1:T(8,128)(2,1)}, u32[]{:S(2)}) copy-start(bf16[2048,192]{0,1:T(8,128)(2,1)} %param.26) | copy-start | bytes 2359300
  34.1 1.3 %copy-start.4 = (bf16[1,2048]{1,0:T(2,128)(2,1)S(1)}, bf16[1,2048]{1,0:T(2,128)(2,1)}, u32[]{:S(2)}) copy-start(bf16[1,2048]{1,0:T(2,128)(2,1)} %get-tuple-element.9) | copy-start | bytes 12292
  35.5 0.7 %copy-start.5 = (bf16[4,544]{1,0:T(4,128)(2,1)S(1)}, bf16[4,544]{1,0:T(4,128)(2,1)}, u32[]{:S(2)}) copy-start(bf16[4,544]{1,0:T(4,128)(2,1)} %get-tuple-element.10) | copy-start | bytes 13060
  36.2 0.7 %copy-start.7 = (bf16[1,544]{1,0:T(2,128)(2,1)S(1)}, bf16[1,544]{1,0:T(2,128)(2,1)}, u32[]{:S(2)}) copy-start(bf16[1,544]{1,0:T(2,128)(2,1)} %get-tuple-element.11) | copy-start | bytes 3268

commit v2 on v1

--- a/solution.py
+++ b/solution.py
@@ -35,8 +35,8 @@
     m,
     pt_h,
     dt_h,
-    pfill,
-    dfill,
+    pf_h,
+    df_h,
     pc_h,
     dc_h,
     ig_h,
@@ -56,6 +56,8 @@
     dr_ref,
     tok,
     dtok,
+    pfill,
+    dfill,
     kbuf,
     dbuf,
     ig,
@@ -90,20 +92,22 @@
     width = tok.shape[2]
     own = vbuf.shape[0]
     rows = x.shape[0]
-    cache = pc_h.shape[0]
-    slots = dc_h.shape[1]
+    cache = pc_h.shape[1]
+    slots = dc_h.shape[2]
     heads = ku.shape[0]
     kl = ku.shape[2]
-    key_width = kbuf.shape[1]
-    part_q = qd.shape[1]
+    key_width = kbuf.shape[0]
+    part_q = qd.shape[0]
     ql = qu.shape[0]
-    extra = kbuf.shape[0] - cache
+    extra = lx.shape[1]
     chunk = obuf.shape[3]
     chunks = obuf.shape[1]
 
     pairs = [
         (pt_h, tok.at[0]),
         (dt_h, dtok),
+        (pf_h, pfill),
+        (df_h, dfill),
         (ig_h, ig),
         (qd_h, qd),
         (ld_h, ld),
@@ -113,15 +117,15 @@
         (qu_h, qu),
         (ru_h, ru),
         (ku_h, ku),
-        (pc_h, kbuf.at[pl.ds(0, cache)]),
+        (pc_h, kbuf),
         (vu_h, vu),
-        (dc_h, dbuf.at[:, pl.ds(0, slots)]),
+        (dc_h, dbuf),
         (op_h, op),
     ]
     loads = [pltpu.make_async_copy(s, d, in_sem.at[i]) for i, (s, d) in enumerate(pairs)]
     for load in loads:
         load.start()
-    l_pt, l_dt, l_ig, l_qd, l_ld, l_rd, l_qg, l_lg, l_qu, l_ru, l_ku, l_pc, l_vu, l_dc, l_op = loads
+    l_pt, l_dt, l_pf, l_df, l_ig, l_qd, l_ld, l_rd, l_qg, l_lg, l_qu, l_ru, l_ku, l_pc, l_vu, l_dc, l_op = loads
 
     barrier = pltpu.get_barrier_semaphore()
     for d in range(1, n):
@@ -148,6 +152,8 @@
         copy.start()
         tok_copies.append(copy)
 
+    l_pf.wait()
+    l_df.wait()
     fill = pfill[0]
     row = lax.broadcasted_iota(jnp.int32, (rows, 1), 0)
     slot = jnp.zeros((rows, 1), jnp.int32)
@@ -184,7 +190,7 @@
     normed = (
         xs * lax.rsqrt(jnp.mean(xs * xs, axis=-1, keepdims=True) + RMS_EPS) * ig[...]
     ).astype(BF16)
-    qx[mt] = dot(normed, qd[...]).astype(BF16)
+    qx[mt] = dot_t(normed, qd[...]).astype(BF16)
     lx[mt] = dot(normed[0:extra], ld[...]).astype(BF16)
 
     a_copies = []
@@ -202,7 +208,7 @@
             copy.start()
             a_copies.append(copy)
 
-    raw = dot(normed[0:extra], rd[...]).astype(BF16).astype(F32)
+    raw = dot_t(normed[0:extra], rd[...]).astype(BF16).astype(F32)
     cos_own = cosine[0:extra, 0:half]
     sin_own = sine[0:extra, 0:half]
     first, second = raw[:, 0:half], raw[:, half:ROPE]
@@ -211,7 +217,7 @@
     )
     for load in (l_qg, l_lg, l_qu, l_ru, l_ku, l_pc, l_vu, l_dc):
         load.wait()
-    gains = qg[...]
+    gains = qg[...].reshape(1, ql)
     for copy in a_copies:
         copy.wait_recv()
 
@@ -240,14 +246,23 @@
     )
     new_rows = jnp.concatenate([latent, new_rope], axis=1)
     new_bf = new_rows.astype(BF16)
-    kbuf[cache : cache + extra, :] = new_bf
+    new_latent, new_key = new_bf[:, 0:kl], new_bf[:, kl:key_width]
     pr_ref[...] = new_rows[0:p].astype(BF16)
     dr_ref[...] = new_rows[p : p + dd].astype(BF16)
 
     score_scale = (NOPE + ROPE) ** (-0.5)
     aq = jnp.concatenate([v.astype(BF16) for v in absorbed], axis=0)
     tq = jnp.concatenate([v.astype(BF16) for v in turned], axis=0)
-    scores = (dot_t(aq, kbuf[:, 0:kl]) + dot_t(tq, kbuf[:, kl:key_width])) * score_scale
+    scores = (
+        jnp.concatenate(
+            [
+                dot(aq, kbuf[0:kl]) + dot(tq, kbuf[kl:key_width]),
+                dot_t(aq, new_latent) + dot_t(tq, new_key),
+            ],
+            axis=1,
+        )
+        * score_scale
+    )
     key = lax.broadcasted_iota(jnp.int32, scores.shape, 1)
     query_place = jnp.concatenate([places] * heads, axis=0)
     fresh = key - cache
@@ -258,13 +273,16 @@
     peak = jnp.max(scores, axis=-1, keepdims=True)
     weights = jnp.where(allowed, jnp.exp(scores - peak), 0.0)
     total = jnp.sum(weights, axis=-1, keepdims=True)
-    mixed = dot(weights.astype(BF16), kbuf[:, 0:kl]).astype(BF16)
-    vd = vu.shape[2]
+    weights = weights.astype(BF16)
+    mixed = (
+        dot_t(weights[:, 0:cache], kbuf[0:kl]) + dot(weights[:, cache:], new_latent)
+    ).astype(BF16)
+    vd = vu.shape[1]
     stat_lane = lax.broadcasted_iota(jnp.int32, (rows, crecv.shape[2] - vd), 1)
     for h in range(heads):
         cut = slice(h * rows, (h + 1) * rows)
         stats = jnp.where(stat_lane == 0, total[cut], peak[cut])
-        message = jnp.concatenate([dot(mixed[cut], vu[h]), stats], axis=1)
+        message = jnp.concatenate([dot_t(mixed[cut], vu[h]), stats], axis=1)
         csend[0, h * p : (h + 1) * p, :] = message[0:p]
         for d in range(1, n):
             start = own + (d - 1) * p
@@ -285,19 +303,28 @@
 
     vbuf[...] = jnp.zeros_like(vbuf)
     for b in range(dd):
-        dbuf[b, slots : slots + extra, :] = new_bf
         at = slice(p + b, p + b + 1)
         qa = jnp.concatenate([v[at] for v in absorbed], axis=0).astype(BF16)
         qt = jnp.concatenate([v[at] for v in turned], axis=0).astype(BF16)
-        ds = (dot_t(qa, dbuf[b, :, 0:kl]) + dot_t(qt, dbuf[b, :, kl:key_width])) * score_scale
+        ds = (
+            jnp.concatenate(
+                [
+                    dot(qa, dbuf[b, 0:kl]) + dot(qt, dbuf[b, kl:key_width]),
+                    dot_t(qa, new_latent) + dot_t(qt, new_key),
+                ],
+                axis=1,
+            )
+            * score_scale
+        )
         dk = lax.broadcasted_iota(jnp.int32, ds.shape, 1)
         ok = (dk < jnp.minimum(dfill[b], slots)) | (dk == slots + p + b)
         ds = jnp.where(ok, ds, NEG_FILL)
         dpeak = jnp.max(ds, axis=-1, keepdims=True)
         dw = jnp.where(ok, jnp.exp(ds - dpeak), 0.0)
         dtotal = jnp.sum(dw, axis=-1, keepdims=True)
-        dmix = dot(dw.astype(BF16), dbuf[b, :, 0:kl]).astype(BF16)
-        dvals = [dot(dmix, vu[h])[h : h + 1] / dtotal[h : h + 1] for h in range(heads)]
+        dw = dw.astype(BF16)
+        dmix = (dot_t(dw[:, 0:slots], dbuf[b, 0:kl]) + dot(dw[:, slots:], new_latent)).astype(BF16)
+        dvals = [dot_t(dmix, vu[h])[h : h + 1] / dtotal[h : h + 1] for h in range(heads)]
         vbuf[p + b : p + b + 1, :] = jnp.concatenate(dvals, axis=1)
     l_op.wait()
 
@@ -347,25 +374,26 @@
     extra = round_up(own, 16)
     heads, nd, kl = ku.shape
     chunks = 2
-    any_spec = pl.BlockSpec(memory_space=pl.ANY)
-    smem = pl.BlockSpec(memory_space=pltpu.SMEM)
+    any_spec = pl.BlockSpec(memory_space=pltpu.HBM)
     vmem = pl.BlockSpec(memory_space=pltpu.VMEM)
-    ig, qg, lg = ig[None], qg[None], lg[None]
+    ig, lg = ig[None], lg[None]
+    pc, qd, rd = pc.T, qd.T, rd.T
+    dc, vu = jnp.swapaxes(dc, 1, 2), jnp.swapaxes(vu, 1, 2)
     like = lambda a: pltpu.VMEM(a.shape, a.dtype)
     scratch = [
         pltpu.VMEM((n, p, width), BF16),
         like(dt),
-        pltpu.VMEM((pc.shape[0] + extra, pc.shape[1]), BF16),
-        pltpu.VMEM((dd, dc.shape[1] + extra, dc.shape[2]), BF16),
-        *[like(a) for a in (ig, qg, lg, qd, ld, rd, qu, ru, ku, vu, op)],
+        pltpu.SMEM(pfill.shape, jnp.int32),
+        pltpu.SMEM(dfill.shape, jnp.int32),
+        *[like(a) for a in (pc, dc, ig, qg, lg, qd, ld, rd, qu, ru, ku, vu, op)],
         pltpu.VMEM((rows, width), F32),
-        pltpu.VMEM((m, rows, qd.shape[1]), BF16),
+        pltpu.VMEM((m, rows, qd.shape[0]), BF16),
         pltpu.VMEM((m, extra, ld.shape[1]), BF16),
         pltpu.VMEM((n, heads * p, 128), F32),
         pltpu.VMEM((n, heads * p, 128), F32),
         pltpu.VMEM((own, op.shape[0]), F32),
         pltpu.VMEM((m, chunks, own, width // chunks), BF16),
-        pltpu.SemaphoreType.DMA((15,)),
+        pltpu.SemaphoreType.DMA((17,)),
         pltpu.SemaphoreType.DMA((2, n)),
         pltpu.SemaphoreType.DMA((2, m)),
         pltpu.SemaphoreType.DMA((2, m)),
@@ -377,10 +405,10 @@
         out_shape=(
             jax.ShapeDtypeStruct((p, width), BF16),
             jax.ShapeDtypeStruct((dd, width), BF16),
-            jax.ShapeDtypeStruct((p, pc.shape[1]), BF16),
-            jax.ShapeDtypeStruct((dd, pc.shape[1]), BF16),
+            jax.ShapeDtypeStruct((p, pc.shape[0]), BF16),
+            jax.ShapeDtypeStruct((dd, pc.shape[0]), BF16),
         ),
-        in_specs=[any_spec, any_spec, smem, smem] + [any_spec] * 13,
+        in_specs=[any_spec] * 17,
         out_specs=(vmem,) * 4,
         scratch_shapes=scratch,
         compiler_params=pltpu.CompilerParams(

time: 37.8 us -> 31 us (0.82)
  local copies, waits for them, and re-layouts: 10.4 us -> 3.29 us
    unnamed x25 -> x10, local copies, waits for them, and re-layouts: 9.81 us -> 3.29 us
    broadcast_in_dim x1 -> x0, local copies, waits for them, and re-layouts: 0.58 us -> none  [local(): ig, qg, lg = (ig[None], qg[None], lg[None])]
where the time goes in v2:
time: 31 us; the launch traced here: 30.6 us
  Pallas kernels  25.4 us (82%)
  local copies, waits for them, and re-layouts  3.29 us (11%)
  between operations  1.95 us (6%)
    pallas_call x1, Pallas kernels, local(): pl.pallas_call(functools.partial(kernel, n, m), out_shape=(jax.ShapeDtype...  25.4 us
    unnamed x10, local copies, waits for them, and re-layouts  3.29 us

profile of v2, /device:TPU:0, one launch (start us, length us, event | category | flops | bytes accessed | tf_op | source)
XLA Modules:
  0.0 30.6 jit_solution(15165908650547472145)
XLA Ops:
  1.9 25.4 %shard_map.192 = (bf16[4,2048]{1,0:T(4,128)(2,1)}, bf16[1,2048]{1,0:T(2,128)(2,1)}, bf16[4,544]{1,0:T(4,128)(2,1)}, bf16[1,544]{1,0:T(2,128)(2,1)}) custom-call(bf16[4,2048]{1,0:T(4,128)(2,1)} %pt_h.1, bf16[1,2048]{1,0:T(2,128)(2,1)} %dt_h.1, s32[1]{0:T(128)S(6)} %copy.25.pf_h, s32[1]{0:T(128)S(6)} %copy.26.df_h, bf16[544,256]{1,0:T(8,128)(2,1)} %bitcast.9, ...), custom_call_target="tpu_custom_call" | custom-call | tf_op jit(solution)/shard_map/pallas_call | solution.py:403
  27.3 0.0 copy-start
  27.3 1.3 %copy.27 = bf16[4,2048]{1,0:T(4,128)(2,1)} copy(bf16[4,2048]{1,0:T(4,128)(2,1)} %get-tuple-element.8) | data formatting | bytes 32768
  28.6 0.0 copy-done
  28.6 0.0 copy-start.1
  28.6 0.6 %copy.28 = bf16[1,2048]{1,0:T(2,128)(2,1)} copy(bf16[1,2048]{1,0:T(2,128)(2,1)S(1)} %copy-done) | data formatting | bytes 8192
  29.2 0.1 copy-done.1
  29.3 0.0 copy-start.2
  29.3 0.6 %copy.29 = bf16[4,544]{1,0:T(4,128)(2,1)} copy(bf16[4,544]{1,0:T(4,128)(2,1)S(1)} %copy-done.1) | data formatting | bytes 8704
  29.9 0.1 copy-done.2
  30.0 0.6 %copy.30 = bf16[1,544]{1,0:T(2,128)(2,1)} copy(bf16[1,544]{1,0:T(2,128)(2,1)S(1)} %copy-done.2) | data formatting | bytes 2176
Async XLA Ops:
  27.3 1.3 %copy-start = (bf16[1,2048]{1,0:T(2,128)(2,1)S(1)}, bf16[1,2048]{1,0:T(2,128)(2,1)}, u32[]{:S(2)}) copy-start(bf16[1,2048]{1,0:T(2,128)(2,1)} %get-tuple-element.9) | copy-start | bytes 12292
  28.6 0.7 %copy-start.1 = (bf16[4,544]{1,0:T(4,128)(2,1)S(1)}, bf16[4,544]{1,0:T(4,128)(2,1)}, u32[]{:S(2)}) copy-start(bf16[4,544]{1,0:T(4,128)(2,1)} %get-tuple-element.10) | copy-start | bytes 13060
  29.3 0.7 %copy-start.2 = (bf16[1,544]{1,0:T(2,128)(2,1)S(1)}, bf16[1,544]{1,0:T(2,128)(2,1)}, u32[]{:S(2)}) copy-start(bf16[1,544]{1,0:T(2,128)(2,1)} %get-tuple-element.11) | copy-start | bytes 3268

commit v3 on v2

v3 whole, which is shorter than its diff:
```python
import functools
import math

import jax
import jax.numpy as jnp
from jax import lax
from jax.experimental import pallas as pl
from jax.experimental.pallas import tpu as pltpu
from jax.sharding import PartitionSpec as P

NOPE = 64
ROPE = 32
NEG_FILL = -1e30
RMS_EPS = 1e-06
THETA = 10000.0
F32 = jnp.float32
BF16 = jnp.bfloat16
MESH = pl.DeviceIdType.MESH


def dot(a, b):
    return jnp.dot(a, b, preferred_element_type=F32)


def dot_t(a, b):
    return lax.dot_general(a, b, (((1,), (1,)), ((), ())), preferred_element_type=F32)


def each(low, high, body):
    if high - low <= 8:
        for i in range(low, high):
            body(i)
    else:
        lax.fori_loop(low, high, lambda i, carry: (body(i), carry)[1], 0)


def round_up(value, step):
    return -(-value // step) * step


def kernel(
    n,
    m,
    pt_h,
    dt_h,
    pf_h,
    df_h,
    pc_h,
    dc_h,
    ig_h,
    qg_h,
    lg_h,
    qd_h,
    ld_h,
    rd_h,
    qu_h,
    ru_h,
    ku_h,
    vu_h,
    op_h,
    po_ref,
    do_ref,
    pr_ref,
    dr_ref,
    tok,
    dtok,
    pfill,
    dfill,
    kbuf,
    dbuf,
    ig,
    qg,
    lg,
    qd,
    ld,
    rd,
    qu,
    ru,
    ku,
    vu,
    op,
    x,
    qall,
    lx,
    qx,
    stage,
    csend,
    crecv,
    dbuf_out,
    outs,
    in_sem,
    q_sem,
    l_sem,
    c_sem,
    d_sem,
    o_sem,
):
    me = lax.axis_index("kv")
    mt = lax.axis_index("tp")
    p = tok.shape[0]
    dd = dtok.shape[0]
    own = lx.shape[1]
    extra = x.shape[0]
    rows = qx.shape[1]
    cache = pc_h.shape[1]
    slots = dc_h.shape[2]
    heads = ku.shape[0]
    kl = ku.shape[2]
    key_width = kbuf.shape[0]
    part_q = qd.shape[0]
    part_l = ld.shape[1]
    ql = qu.shape[0]
    chunks = len(outs)
    chunk = outs[0].shape[2]

    pairs = [
        (pt_h, tok),
        (dt_h, dtok),
        (ig_h, ig),
        (qd_h, qd),
        (ld_h, ld),
        (rd_h, rd),
        (pf_h, pfill),
        (df_h, dfill),
        (qg_h, qg),
        (lg_h, lg),
        (qu_h, qu),
        (ru_h, ru),
        (ku_h, ku),
        (pc_h, kbuf),
        (vu_h, vu),
        (dc_h, dbuf),
        (op_h, op),
    ]
    loads = [pltpu.make_async_copy(s, d, in_sem.at[i]) for i, (s, d) in enumerate(pairs)]
    for load in loads:
        load.start()
    early, late, last = loads[:6], loads[6:-1], loads[-1]

    barrier = pltpu.get_barrier_semaphore()

    def greet(dk, dt):
        pl.semaphore_signal(
            barrier,
            inc=1,
            device_id=(lax.rem(me + dk, n), lax.rem(mt + dt, m)),
            device_id_type=MESH,
        )

    for dt in range(m):
        each(0 if dt else 1, n, lambda dk, dt=dt: greet(dk, dt))

    x[...] = jnp.zeros_like(x)
    for load in early:
        load.wait()
    x[0:p, :] = tok[...].astype(F32)
    x[p : p + dd, :] = dtok[...].astype(F32)
    xs = x[...]
    normed = (
        xs * lax.rsqrt(jnp.mean(xs * xs, axis=-1, keepdims=True) + RMS_EPS) * ig[...]
    ).astype(BF16)
    columns = dot_t(normed, qd[...])[0:own]
    qall[mt, 0] = columns[0:p].astype(BF16)
    lx[mt] = jnp.concatenate([dot(normed, ld[...])[0:own], columns], axis=1).astype(BF16)
    raw = dot_t(normed, rd[...])[0:own].astype(BF16).astype(F32)

    pl.semaphore_wait(barrier, n * m - 1)

    def query_copy(dk, dt):
        return pltpu.make_async_remote_copy(
            src_ref=qall.at[mt, 0],
            dst_ref=qall.at[mt, dk],
            send_sem=q_sem.at[0, dt, dk],
            recv_sem=q_sem.at[1, dt, dk],
            device_id=(lax.rem(me + dk, n), lax.rem(mt + dt, m)),
            device_id_type=MESH,
        )

    for dt in range(m):
        each(1, n, lambda dk, dt=dt: query_copy(dk, dt).start())
    l_copies = []
    for dt in range(1, m):
        copy = pltpu.make_async_remote_copy(
            src_ref=lx.at[mt],
            dst_ref=lx.at[mt],
            send_sem=l_sem.at[0, dt],
            recv_sem=l_sem.at[1, dt],
            device_id=(me, lax.rem(mt + dt, m)),
            device_id_type=MESH,
        )
        copy.start()
        l_copies.append(copy)

    for load in late:
        load.wait()
    fill = pfill[...]
    row = lax.broadcasted_iota(jnp.int32, (rows, 1), 0)
    slot = jnp.zeros((rows, 1), jnp.int32)
    for d in range(1, n):
        slot = jnp.where(row >= own + (d - 1) * p, d, slot)
    source = me - slot
    source = jnp.where(source < 0, source + n, source)
    inside = jnp.where(slot == 0, row, row - own - (slot - 1) * p)
    places = fill + source * p + inside
    for b in range(dd):
        places = jnp.where(row == p + b, dfill[b : b + 1, :], places)
    half = ROPE // 2
    turned_axis = heads * ROPE
    lane = lax.broadcasted_iota(jnp.int32, (1, turned_axis), 1)
    frequency = jnp.zeros((1, turned_axis), F32)
    for i in range(half):
        frequency = jnp.where(lane % half == i, THETA ** (-i / half), frequency)
    angles = places.astype(F32) * frequency
    cosine = jnp.cos(angles)
    sine = jnp.sin(angles)
    cos_own = cosine[0:own, 0:half]
    sin_own = sine[0:own, 0:half]
    first, second = raw[:, 0:half], raw[:, half:ROPE]
    new_rope = jnp.concatenate(
        [first * cos_own - second * sin_own, first * sin_own + second * cos_own], axis=1
    )
    gains = qg[...].reshape(1, ql)
    qx[...] = jnp.zeros_like(qx)

    for copy in l_copies:
        copy.wait_recv()
    latent = jnp.concatenate([lx[s, :, 0:part_l].astype(F32) for s in range(m)], axis=1)
    latent = (
        latent * lax.rsqrt(jnp.mean(latent * latent, axis=-1, keepdims=True) + RMS_EPS) * lg[...]
    )
    new_rows = jnp.concatenate([latent, new_rope], axis=1)
    pr_ref[...] = new_rows[0:p].astype(BF16)
    dr_ref[...] = new_rows[p : p + dd].astype(BF16)
    new_bf = jnp.concatenate([new_rows, jnp.zeros((extra - own, key_width), F32)], axis=0)
    new_bf = new_bf.astype(BF16)
    new_latent, new_key = new_bf[:, 0:kl], new_bf[:, kl:key_width]
    for s in range(m):
        qx[s, 0:own, :] = lx[s, :, part_l:].astype(F32)

    for dt in range(m):
        each(1, n, lambda dk, dt=dt: query_copy(dk, dt).wait_recv())
    for d in range(1, n):
        start = own + (d - 1) * p
        qx[:, start : start + p, :] = qall[:, d].astype(F32)
    parts = [qx[s] for s in range(m)]
    square = sum(jnp.sum(v * v, axis=-1, keepdims=True) for v in parts)
    scale = lax.rsqrt(square / ql + RMS_EPS)
    nope = jnp.zeros((rows, qu.shape[1]), F32)
    turn = jnp.zeros((rows, ru.shape[1]), F32)
    for s in range(m):
        lat = (parts[s] * scale * gains[:, s * part_q : (s + 1) * part_q]).astype(BF16)
        nope += dot(lat, qu[s * part_q : (s + 1) * part_q, :])
        turn += dot(lat, ru[s * part_q : (s + 1) * part_q, :])
    nope = nope.astype(BF16)
    turn = turn.astype(BF16).astype(F32)
    above = pltpu.roll(turn, turned_axis - half, 1)
    below = pltpu.roll(turn, half, 1)
    turned = turn * cosine + jnp.where(lane % ROPE < half, -above, below) * sine
    nd = qu.shape[1] // heads
    absorbed = [dot(nope[:, h * nd : (h + 1) * nd], ku[h]) for h in range(heads)]
    turned = [turned[:, h * ROPE : (h + 1) * ROPE] for h in range(heads)]

    score_scale = (NOPE + ROPE) ** (-0.5)
    aq = jnp.concatenate(absorbed, axis=0).astype(BF16)
    tq = jnp.concatenate(turned, axis=0).astype(BF16)
    scores = (
        jnp.concatenate(
            [
                dot(aq, kbuf[0:kl]) + dot(tq, kbuf[kl:key_width]),
                dot_t(aq, new_latent) + dot_t(tq, new_key),
            ],
            axis=1,
        )
        * score_scale
    )
    key = lax.broadcasted_iota(jnp.int32, (1, cache + extra), 1)
    query_place = jnp.concatenate([places] * heads, axis=0)
    fresh = key - cache
    never = jnp.int32(2**30)
    stored = jnp.where(me * cache + key < fill, me * cache + key, never)
    key_place = jnp.where(fresh < 0, stored, jnp.where(fresh < p, fill + me * p + fresh, never))
    allowed = key_place <= query_place
    scores = jnp.where(allowed, scores, NEG_FILL)
    peak = jnp.max(scores, axis=-1, keepdims=True)
    weights = jnp.where(allowed, jnp.exp(scores - peak), 0.0)
    total = jnp.sum(weights, axis=-1, keepdims=True)
    weights = weights.astype(BF16)
    mixed = dot_t(weights[:, 0:cache], kbuf[0:kl]) + dot(weights[:, cache:], new_latent)
    vd = vu.shape[1]
    peak_high = peak.astype(BF16).astype(F32)
    peak_mid = (peak - peak_high).astype(BF16).astype(F32)
    peak_low = peak - peak_high - peak_mid
    total_high = total.astype(BF16).astype(F32)
    total_low = total - total_high
    stat_lane = lax.broadcasted_iota(jnp.int32, (1, csend.shape[2] - vd), 1)
    stats = jnp.where(stat_lane == 0, peak_high, total_low)
    stats = jnp.where(stat_lane == 1, peak_mid, stats)
    stats = jnp.where(stat_lane == 2, peak_low, stats)
    stats = jnp.where(stat_lane == 3, total_high, stats)
    for h in range(heads):
        cut = slice(h * rows, (h + 1) * rows)
        message = jnp.concatenate([dot_t(mixed[cut].astype(BF16), vu[h]), stats[cut]], axis=1)
        stage[0, h * p : (h + 1) * p, :] = message[0:p]
        for d in range(1, n):
            start = own + (d - 1) * p
            stage[d, h * p : (h + 1) * p, :] = message[start : start + p]
    csend[...] = stage[...].astype(BF16)

    def value_copy(d):
        return pltpu.make_async_remote_copy(
            src_ref=csend.at[d],
            dst_ref=crecv.at[d],
            send_sem=c_sem.at[0, d],
            recv_sem=c_sem.at[1, d],
            device_id=(lax.rem(me + n - d, n), mt),
            device_id_type=MESH,
        )

    each(1, n, lambda d: value_copy(d).start())

    dvalues = []
    for b in range(dd):
        at = slice(p + b, p + b + 1)
        qa = jnp.concatenate([v[at] for v in absorbed], axis=0).astype(BF16)
        qt = jnp.concatenate([v[at] for v in turned], axis=0).astype(BF16)
        ds = (
            jnp.concatenate(
                [
                    dot(qa, dbuf[b, 0:kl]) + dot(qt, dbuf[b, kl:key_width]),
                    dot_t(qa, new_latent) + dot_t(qt, new_key),
                ],
                axis=1,
            )
            * score_scale
        )
        dk = lax.broadcasted_iota(jnp.int32, ds.shape, 1)
        ok = (dk < jnp.minimum(dfill[b : b + 1, :], slots)) | (dk == slots + p + b)
        ds = jnp.where(ok, ds, NEG_FILL)
        dpeak = jnp.max(ds, axis=-1, keepdims=True)
        dw = jnp.where(ok, jnp.exp(ds - dpeak), 0.0)
        dtotal = jnp.sum(dw, axis=-1, keepdims=True)
        dw = dw.astype(BF16)
        dmix = (dot_t(dw[:, 0:slots], dbuf[b, 0:kl]) + dot(dw[:, slots:], new_latent)).astype(BF16)
        dvals = [dot_t(dmix, vu[h])[h : h + 1] / dtotal[h : h + 1] for h in range(heads)]
        dvalues.append(jnp.concatenate(dvals, axis=1))
    last.wait()

    def row_copy(buf, sem, dt):
        return pltpu.make_async_remote_copy(
            src_ref=buf.at[mt],
            dst_ref=buf.at[mt],
            send_sem=sem.at[0, dt],
            recv_sem=sem.at[1, dt],
            device_id=(me, lax.rem(mt + dt, m)),
            device_id_type=MESH,
        )

    dbuf_out[mt] = dot(jnp.concatenate(dvalues, axis=0).astype(BF16), op[...]).astype(BF16)
    o_copies = [row_copy(dbuf_out, d_sem, dt) for dt in range(1, m)]
    for copy in o_copies:
        copy.start()

    each(1, n, lambda d: value_copy(d).wait_recv())
    blocks = [csend[0].astype(F32)] + [crecv[d].astype(F32) for d in range(1, n)]

    def peak_of(block):
        return block[:, vd : vd + 1] + block[:, vd + 1 : vd + 2] + block[:, vd + 2 : vd + 3]

    peaks = [peak_of(block) for block in blocks]
    top = functools.reduce(jnp.maximum, peaks)
    merged = jnp.zeros(blocks[0].shape, F32)
    for block, block_peak in zip(blocks, peaks):
        merged += block * jnp.exp(block_peak - top)
    value = merged[:, 0:vd] / (merged[:, vd + 3 : vd + 4] + merged[:, vd + 4 : vd + 5])
    values = jnp.concatenate([value[h * p : (h + 1) * p] for h in range(heads)], axis=1)
    values = values.astype(BF16)
    for c in range(chunks):
        obuf = outs[c]
        obuf[mt] = dot(values, op[:, c * chunk : (c + 1) * chunk]).astype(BF16)
        for dt in range(1, m):
            copy = row_copy(obuf, o_sem.at[c], dt)
            copy.start()
            o_copies.append(copy)
    for copy in o_copies:
        copy.wait_recv()
    do_ref[...] = sum(dbuf_out[s].astype(F32) for s in range(m)).astype(BF16)
    for c in range(chunks):
        out = sum(outs[c][s].astype(F32) for s in range(m))
        po_ref[:, c * chunk : (c + 1) * chunk] = out.astype(BF16)
    for dt in range(m):
        each(1, n, lambda dk, dt=dt: query_copy(dk, dt).wait_send())
    each(1, n, lambda d: value_copy(d).wait_send())
    for copy in l_copies + o_copies:
        copy.wait_send()


def local(n, m, *args):
    (pt, dt, pfill, dfill, pc, dc, ig, qg, lg, qd, ld, rd, qu, ru, ku, vu, op) = args
    p, width = pt.shape
    dd = dt.shape[0]
    own = round_up(p + dd, 8)
    rows = round_up(own + (n - 1) * p, 8)
    extra = round_up(own, 16)
    heads, nd, kl = ku.shape
    chunks = 2
    any_spec = pl.BlockSpec(memory_space=pltpu.HBM)
    vmem = pl.BlockSpec(memory_space=pltpu.VMEM)
    ig, lg = ig[None], lg[None]
    pfill, dfill = pfill[None], dfill[:, None]
    pc, qd, rd = pc.T, qd.T, rd.T
    dc, vu = jnp.swapaxes(dc, 1, 2), jnp.swapaxes(vu, 1, 2)
    like = lambda a: pltpu.VMEM(a.shape, a.dtype)
    scratch = [
        *[like(a) for a in (pt, dt, pfill, dfill, pc, dc, ig, qg, lg)],
        *[like(a) for a in (qd, ld, rd, qu, ru, ku, vu, op)],
        pltpu.VMEM((extra, width), F32),
        pltpu.VMEM((m, n, p, qd.shape[0]), BF16),
        pltpu.VMEM((m, own, ld.shape[1] + qd.shape[0]), BF16),
        pltpu.VMEM((m, rows, qd.shape[0]), F32),
        pltpu.VMEM((n, heads * p, 128), F32),
        pltpu.VMEM((n, heads * p, 128), BF16),
        pltpu.VMEM((n, heads * p, 128), BF16),
        pltpu.VMEM((m, dd, width), BF16),
        [pltpu.VMEM((m, p, width // chunks), BF16)] * chunks,
        pltpu.SemaphoreType.DMA((17,)),
        pltpu.SemaphoreType.DMA((2, m, n)),
        pltpu.SemaphoreType.DMA((2, m)),
        pltpu.SemaphoreType.DMA((2, n)),
        pltpu.SemaphoreType.DMA((2, m)),
        pltpu.SemaphoreType.DMA((chunks, 2, m)),
    ]
    return pl.pallas_call(
        functools.partial(kernel, n, m),
        out_shape=(
            jax.ShapeDtypeStruct((p, width), BF16),
            jax.ShapeDtypeStruct((dd, width), BF16),
            jax.ShapeDtypeStruct((p, pc.shape[0]), BF16),
            jax.ShapeDtypeStruct((dd, pc.shape[0]), BF16),
        ),
        in_specs=[any_spec] * 17,
        out_specs=(vmem,) * 4,
        scratch_shapes=scratch,
        compiler_params=pltpu.CompilerParams(
            collective_id=0, has_side_effects=True, vmem_limit_bytes=60 * 1024 * 1024
        ),
    )(pt, dt, pfill, dfill, pc, dc, ig, qg, lg, qd, ld, rd, qu, ru, ku, vu, op)


def solution(mesh):
    placed = (
        P("kv", None),
        P("kv", None),
        P(),
        P("kv"),
        P("kv", None),
        P("kv", None, None),
        P(),
        P(),
        P(),
        P(None, "tp"),
        P(None, "tp"),
        P(),
        P(None, "tp"),
        P(None, "tp"),
        P("tp", None, None),
        P("tp", None, None),
        P("tp", None),
    )
    return jax.shard_map(
        functools.partial(local, mesh.shape["kv"], mesh.shape["tp"]),
        mesh=mesh,
        in_specs=placed,
        out_specs=(P("kv", None), P("kv", None), P("kv", None), P("kv", None)),
        check_vma=False,
    )
```

time: 31 us -> 28.2 us (0.910)
  Pallas kernels: 25.4 us -> 22.6 us
    pallas_call x1, Pallas kernels: 25.4 us -> 22.6 us  [local(): pl.pallas_call(functools.partial(kernel, n, m), out_shape=(jax.ShapeDtype...]
where the time goes in v3:
time: 28.2 us; the launch traced here: 27.8 us
  Pallas kernels  22.6 us (80%)
  local copies, waits for them, and re-layouts  3.29 us (12%)
  between operations  1.95 us (7%)
    pallas_call x1, Pallas kernels, local(): pl.pallas_call(functools.partial(kernel, n, m), out_shape=(jax.ShapeDtype...  22.6 us
    unnamed x10, local copies, waits for them, and re-layouts  3.29 us

profile of v3, /device:TPU:0, one launch (start us, length us, event | category | flops | bytes accessed | tf_op | source)
XLA Modules:
  0.0 27.8 jit_solution(2005690381716009063)
XLA Ops:
  1.9 22.6 %shard_map.192 = (bf16[4,2048]{1,0:T(4,128)(2,1)}, bf16[1,2048]{1,0:T(2,128)(2,1)}, bf16[4,544]{1,0:T(4,128)(2,1)}, bf16[1,544]{1,0:T(2,128)(2,1)}) custom-call(bf16[4,2048]{1,0:T(4,128)(2,1)} %pt_h.1, bf16[1,2048]{1,0:T(2,128)(2,1)} %dt_h.1, s32[1,1]{1,0:T(1,128)} %bitcast.9.pf_h, s32[1,1]{1,0:T(1,128)} %bitcast.10.df_h, bf16[544,256]{1,0:T(8,128)(2,1)} %bitcast.13, ...), custom_call_target="tpu_custom_call" | custom-call | tf_op jit(solution)/shard_map/pallas_call | solution.py:432
  24.5 0.0 copy-start
  24.5 1.3 %copy.27 = bf16[4,2048]{1,0:T(4,128)(2,1)} copy(bf16[4,2048]{1,0:T(4,128)(2,1)} %get-tuple-element.8) | data formatting | bytes 32768
  25.9 0.0 copy-done
  25.9 0.0 copy-start.1
  25.9 0.6 %copy.28 = bf16[1,2048]{1,0:T(2,128)(2,1)} copy(bf16[1,2048]{1,0:T(2,128)(2,1)S(1)} %copy-done) | data formatting | bytes 8192
  26.5 0.1 copy-done.1
  26.6 0.0 copy-start.2
  26.6 0.6 %copy.29 = bf16[4,544]{1,0:T(4,128)(2,1)} copy(bf16[4,544]{1,0:T(4,128)(2,1)S(1)} %copy-done.1) | data formatting | bytes 8704
  27.2 0.1 copy-done.2
  27.2 0.6 %copy.30 = bf16[1,544]{1,0:T(2,128)(2,1)} copy(bf16[1,544]{1,0:T(2,128)(2,1)S(1)} %copy-done.2) | data formatting | bytes 2176
Async XLA Ops:
  24.5 1.3 %copy-start = (bf16[1,2048]{1,0:T(2,128)(2,1)S(1)}, bf16[1,2048]{1,0:T(2,128)(2,1)}, u32[]{:S(2)}) copy-start(bf16[1,2048]{1,0:T(2,128)(2,1)} %get-tuple-element.9) | copy-start | bytes 12292
  25.9 0.7 %copy-start.1 = (bf16[4,544]{1,0:T(4,128)(2,1)S(1)}, bf16[4,544]{1,0:T(4,128)(2,1)}, u32[]{:S(2)}) copy-start(bf16[4,544]{1,0:T(4,128)(2,1)} %get-tuple-element.10) | copy-start | bytes 13060
  26.6 0.7 %copy-start.2 = (bf16[1,544]{1,0:T(2,128)(2,1)S(1)}, bf16[1,544]{1,0:T(2,128)(2,1)}, u32[]{:S(2)}) copy-start(bf16[1,544]{1,0:T(2,128)(2,1)} %get-tuple-element.11) | copy-start | bytes 3268

commit v4 on v3

--- a/solution.py
+++ b/solution.py
@@ -394,6 +394,18 @@
         copy.wait_send()
 
 
+def put_out(*refs):
+    count = len(refs) // 2
+    sem = refs[-1]
+    copies = [
+        pltpu.make_async_copy(refs[i], refs[count + i], sem.at[i]) for i in range(count)
+    ]
+    for copy in copies:
+        copy.start()
+    for copy in copies:
+        copy.wait()
+
+
 def local(n, m, *args):
     (pt, dt, pfill, dfill, pc, dc, ig, qg, lg, qd, ld, rd, qu, ru, ku, vu, op) = args
     p, width = pt.shape
@@ -429,13 +441,13 @@
         pltpu.SemaphoreType.DMA((2, m)),
         pltpu.SemaphoreType.DMA((chunks, 2, m)),
     ]
-    return pl.pallas_call(
+    held = pl.pallas_call(
         functools.partial(kernel, n, m),
         out_shape=(
-            jax.ShapeDtypeStruct((p, width), BF16),
-            jax.ShapeDtypeStruct((dd, width), BF16),
-            jax.ShapeDtypeStruct((p, pc.shape[0]), BF16),
-            jax.ShapeDtypeStruct((dd, pc.shape[0]), BF16),
+            pltpu.VMEM((p, width), BF16),
+            pltpu.VMEM((dd, width), BF16),
+            pltpu.VMEM((p, pc.shape[0]), BF16),
+            pltpu.VMEM((dd, pc.shape[0]), BF16),
         ),
         in_specs=[any_spec] * 17,
         out_specs=(vmem,) * 4,
@@ -444,6 +456,14 @@
             collective_id=0, has_side_effects=True, vmem_limit_bytes=60 * 1024 * 1024
         ),
     )(pt, dt, pfill, dfill, pc, dc, ig, qg, lg, qd, ld, rd, qu, ru, ku, vu, op)
+    return pl.pallas_call(
+        put_out,
+        out_shape=tuple(jax.ShapeDtypeStruct(a.shape, a.dtype) for a in held),
+        in_specs=[vmem] * len(held),
+        out_specs=(any_spec,) * len(held),
+        scratch_shapes=[pltpu.SemaphoreType.DMA((len(held),))],
+        compiler_params=pltpu.CompilerParams(vmem_limit_bytes=1024 * 1024),
+    )(*held)
 
 
 def solution(mesh):

time: 28.2 us -> 24.8 us (0.88)
  local copies, waits for them, and re-layouts: 3.29 us -> 0 us
    unnamed x10 -> x0, local copies, waits for them, and re-layouts: 3.29 us -> none
    pallas_call x1 -> x2, Pallas kernels: 22.6 us -> 22.6 us  [the longest x1 22 us: local(): pl.pallas_call(functools.partial(kernel, n, m), out_shape=(pltpu.VMEM((p,...]
where the time goes in v4:
time: 24.8 us; the launch traced here: 24.5 us
  Pallas kernels  22.6 us (91%)
  between operations  1.94 us (8%)
    pallas_call x1, Pallas kernels, local(): pl.pallas_call(functools.partial(kernel, n, m), out_shape=(pltpu.VMEM((p,...  22 us
    pallas_call x1, Pallas kernels, local(): pl.pallas_call(put_out, out_shape=tuple((jax.ShapeDtypeStruct(a.shape, a....  0.65 us

profile of v4, /device:TPU:0, one launch (start us, length us, event | category | flops | bytes accessed | tf_op | source)
XLA Modules:
  0.0 24.5 jit_solution(10077352728775389231)
XLA Ops:
  1.9 22.0 %shard_map.192 = (bf16[4,2048]{1,0:T(4,128)(2,1)S(1)}, bf16[1,2048]{1,0:T(2,128)(2,1)S(1)}, bf16[4,544]{1,0:T(4,128)(2,1)S(1)}, bf16[1,544]{1,0:T(2,128)(2,1)S(1)}) custom-call(bf16[4,2048]{1,0:T(4,128)(2,1)} %pt_h.1, bf16[1,2048]{1,0:T(2,128)(2,1)} %dt_h.1, s32[1,1]{1,0:T(1,128)} %bitcast.9.pf_h, s32[1,1]{1,0:T(1,128)} %bitcast.10.df_h, ...), custom_call_target="tpu_custom_call" | custom-call | tf_op jit(solution)/shard_map/pallas_call | solution.py:444
  23.9 0.6 %shard_map.193 = (bf16[4,2048]{1,0:T(4,128)(2,1)}, bf16[1,2048]{1,0:T(2,128)(2,1)}, bf16[4,544]{1,0:T(4,128)(2,1)}, bf16[1,544]{1,0:T(2,128)(2,1)}) custom-call(bf16[4,2048]{1,0:T(4,128)(2,1)S(1)} %get-tuple-element.8.refs_0_, bf16[1,2048]{1,0:T(2,128)(2,1)S(1)} %get-tuple-element.9.refs_1_, bf16[4,544]{1,0:T(4,128)(2,1)S(1)} %get-tuple-element.10.refs_2_, ...), custom_call_target="tpu_custom_call" | custom-call | tf_op jit(solution)/shard_map/pallas_call | solution.py:459

commit v5 on v4

--- a/solution.py
+++ b/solution.py
@@ -28,7 +28,7 @@
 
 def each(low, high, body):
     if high - low <= 8:
-        for i in range(low, high):
+        for i in sorted(range(low, high), key=lambda i: -min(i, high - i)):
             body(i)
     else:
         lax.fori_loop(low, high, lambda i, carry: (body(i), carry)[1], 0)
@@ -133,9 +133,9 @@
         (op_h, op),
     ]
     loads = [pltpu.make_async_copy(s, d, in_sem.at[i]) for i, (s, d) in enumerate(pairs)]
-    for load in loads:
+    early, late, last = loads[:6], loads[6:-1], loads[-1]
+    for load in early:
         load.start()
-    early, late, last = loads[:6], loads[6:-1], loads[-1]
 
     barrier = pltpu.get_barrier_semaphore()
 
@@ -153,6 +153,8 @@
     x[...] = jnp.zeros_like(x)
     for load in early:
         load.wait()
+    for load in loads[6:]:
+        load.start()
     x[0:p, :] = tok[...].astype(F32)
     x[p : p + dd, :] = dtok[...].astype(F32)
     xs = x[...]
@@ -176,8 +178,6 @@
             device_id_type=MESH,
         )
 
-    for dt in range(m):
-        each(1, n, lambda dk, dt=dt: query_copy(dk, dt).start())
     l_copies = []
     for dt in range(1, m):
         copy = pltpu.make_async_remote_copy(
@@ -190,6 +190,8 @@
         )
         copy.start()
         l_copies.append(copy)
+    for dt in reversed(range(m)):
+        each(1, n, lambda dk, dt=dt: query_copy(dk, dt).start())
 
     for load in late:
         load.wait()
@@ -381,10 +383,12 @@
             copy = row_copy(obuf, o_sem.at[c], dt)
             copy.start()
             o_copies.append(copy)
-    for copy in o_copies:
+    for copy in o_copies[: m - 1]:
         copy.wait_recv()
     do_ref[...] = sum(dbuf_out[s].astype(F32) for s in range(m)).astype(BF16)
     for c in range(chunks):
+        for copy in o_copies[(c + 1) * (m - 1) : (c + 2) * (m - 1)]:
+            copy.wait_recv()
         out = sum(outs[c][s].astype(F32) for s in range(m))
         po_ref[:, c * chunk : (c + 1) * chunk] = out.astype(BF16)
     for dt in range(m):
@@ -414,7 +418,7 @@
     rows = round_up(own + (n - 1) * p, 8)
     extra = round_up(own, 16)
     heads, nd, kl = ku.shape
-    chunks = 2
+    chunks = 1
     any_spec = pl.BlockSpec(memory_space=pltpu.HBM)
     vmem = pl.BlockSpec(memory_space=pltpu.VMEM)
     ig, lg = ig[None], lg[None]

time: 24.8 us -> 24.6 us (level)
  no operation moved by 1% of the time
where the time goes in v5:
time: 24.6 us; the launch traced here: 24.3 us
  Pallas kernels  22.4 us (91%)
  between operations  1.94 us (8%)
    pallas_call x1, Pallas kernels, local(): pl.pallas_call(functools.partial(kernel, n, m), out_shape=(pltpu.VMEM((p,...  21.7 us
    pallas_call x1, Pallas kernels, local(): pl.pallas_call(put_out, out_shape=tuple((jax.ShapeDtypeStruct(a.shape, a....  0.65 us

profile of v5, /device:TPU:0, one launch (start us, length us, event | category | flops | bytes accessed | tf_op | source)
XLA Modules:
  0.0 24.3 jit_solution(5991958309664366361)
XLA Ops:
  1.9 21.7 %shard_map.192 = (bf16[4,2048]{1,0:T(4,128)(2,1)S(1)}, bf16[1,2048]{1,0:T(2,128)(2,1)S(1)}, bf16[4,544]{1,0:T(4,128)(2,1)S(1)}, bf16[1,544]{1,0:T(2,128)(2,1)S(1)}) custom-call(bf16[4,2048]{1,0:T(4,128)(2,1)} %pt_h.1, bf16[1,2048]{1,0:T(2,128)(2,1)} %dt_h.1, s32[1,1]{1,0:T(1,128)} %bitcast.9.pf_h, s32[1,1]{1,0:T(1,128)} %bitcast.10.df_h, ...), custom_call_target="tpu_custom_call" | custom-call | tf_op jit(solution)/shard_map/pallas_call | solution.py:448
  23.7 0.6 %shard_map.193 = (bf16[4,2048]{1,0:T(4,128)(2,1)}, bf16[1,2048]{1,0:T(2,128)(2,1)}, bf16[4,544]{1,0:T(4,128)(2,1)}, bf16[1,544]{1,0:T(2,128)(2,1)}) custom-call(bf16[4,2048]{1,0:T(4,128)(2,1)S(1)} %get-tuple-element.8.refs_0_, bf16[1,2048]{1,0:T(2,128)(2,1)S(1)} %get-tuple-element.9.refs_1_, bf16[4,544]{1,0:T(4,128)(2,1)S(1)} %get-tuple-element.10.refs_2_, ...), custom_call_target="tpu_custom_call" | custom-call | tf_op jit(solution)/shard_map/pallas_call | solution.py:463
